TPU v7x, 128 devices: a whole 4x4x4 slice. The times are simulated.
128 devices in a mesh: sp: 16 (over z, x), tp: 8 (over y, core).
Axes of the slice: x: 4, y: 4, z: 4, core: 2. Of those that a mesh axis runs over, the one named last changes fastest.
Arguments:
- target: bfloat16 [8192, 4096], P(('sp', 'tp')), may hold values from -0.07 to 0.07
- source: bfloat16 [16384, 4096], P(('sp', 'tp')), may hold values from -0.035 to 0.035
- gain_target: float32 [4096], replicated, may hold values from 0.1 to 1.9
- gain_source: float32 [4096], replicated, may hold values from 0.1 to 1.9
- w_query: bfloat16 [4096, 1024], P(None, 'tp'), may hold values from -1 to 1
- w_key: bfloat16 [4096, 512], replicated, may hold values from -1 to 1
- w_value: bfloat16 [4096, 512], replicated, may hold values from -0.09375 to 0.09375
- w_out: bfloat16 [1024, 4096], P('tp'), may hold values from -0.1875 to 0.1875
- grad_output: bfloat16 [8192, 4096], P(('sp', 'tp')), may hold values from -6 to 6
Outputs:
- grad_target: float32 [8192, 4096], P(('sp', 'tp'))
- grad_source: float32 [16384, 4096], P(('sp', 'tp'))
- grad_out_proj: float32 [1024, 4096], P('tp')
All inputs are finite; a program needn't handle non-finite values.
Results may differ from a plain program's by a relative error of at most 0.028.
Values may be sent and summed in bfloat16 or wider, within the bound.
No kernel may reach another device: no remote copies, remote signals or barrier semaphores. Data moves between devices by JAX's collectives and lax.ppermute only.
A program may use at most 128 MiB of HBM per device.

v0:
```python
import math
import jax
import jax.numpy as jnp
from jax import lax
from jax.sharding import PartitionSpec as P

HD = 64
EPS = 1e-06


def sent_together(arrays, axis, dim, along):
    both = jnp.concatenate(arrays, axis=along)
    whole, at, finished = (lax.all_gather(both, axis, axis=dim, tiled=True), 0, [])
    for a in arrays:
        finished.append(lax.slice_in_dim(whole, at, at + a.shape[along], axis=along))
        at += a.shape[along]
    return tuple(finished)


def normalize(matrix, scaling):
    widened = matrix.astype(jnp.float32)
    factor = lax.rsqrt(jnp.mean(widened * widened, axis=-1, keepdims=True) + EPS)
    return (widened * factor * scaling).astype(jnp.bfloat16)


def norm_back(matrix, scaling, upstream):
    widened = matrix.astype(jnp.float32)
    factor = lax.rsqrt(jnp.mean(widened * widened, axis=-1, keepdims=True) + EPS)
    weighted = upstream * scaling
    inner = jnp.mean(widened * weighted, axis=-1, keepdims=True)
    return factor * weighted - widened * factor * factor * factor * inner


def score_block(queries, key_block, score_scale):
    return (
        jnp.einsum(
            "tkgd,skd->kgts", queries, key_block[:, :, 0], preferred_element_type=jnp.float32
        )
        * score_scale
    )


def split_arrived(arrived, key_count):
    row_count = arrived.shape[0]
    block_size = math.gcd(row_count, 1024)
    return (arrived.reshape(row_count // block_size, block_size, key_count, 2, HD), block_size)


def shards(target, source, gain_target, gain_source, w_query, w_key, w_value, w_out, grad_output):
    contract_last = (((1,), (1,)), ((), ()))
    across = lax.axis_size("tp")
    heads_all = w_key.shape[1] // HD
    key_count = heads_all // across
    query_count = w_query.shape[1] // HD
    group_size = query_count // key_count
    score_scale = float(HD) ** (-0.5)
    normed_target = normalize(target, gain_target)
    normed_source = normalize(source, gain_source)
    gathered_target, gathered_grad = sent_together((normed_target, grad_output), "tp", 0, 1)
    query = jnp.dot(gathered_target, w_query, preferred_element_type=jnp.float32).astype(
        jnp.bfloat16
    )
    head_grads = lax.dot_general(
        gathered_grad, w_out, contract_last, preferred_element_type=jnp.float32
    ).astype(jnp.bfloat16)
    row_count = query.shape[0]
    queries = query.reshape(row_count, key_count, group_size, HD)
    grad_heads = head_grads.reshape(row_count, key_count, group_size, HD)
    w_both = jnp.stack(
        [w_key.reshape(-1, heads_all, HD), w_value.reshape(-1, heads_all, HD)], axis=2
    )
    w_both = w_both.reshape(w_key.shape[0], heads_all * 2 * HD)
    pairs = jnp.dot(normed_source, w_both, preferred_element_type=jnp.float32).astype(jnp.bfloat16)
    own_pairs = lax.all_to_all(pairs, "tp", split_axis=1, concat_axis=0, tiled=True)
    start_max = jnp.full((key_count, group_size, row_count), -jnp.inf, jnp.float32)
    start_sum = jnp.zeros((key_count, group_size, row_count), jnp.float32)
    start_acc = jnp.zeros((row_count, key_count, group_size, HD), jnp.float32)
    blocks, block_size = split_arrived(
        lax.all_gather(own_pairs, "sp", axis=0, tiled=True), key_count
    )

    def absorb_advance(status, key_block):
        maxima, totals, accum = status
        scores = score_block(queries, key_block, score_scale)
        new_max = jnp.maximum(maxima, jnp.max(scores, axis=-1))
        shrink = jnp.exp(maxima - new_max)
        weights = jnp.exp(scores - new_max[..., None])
        totals = totals * shrink + jnp.sum(weights, axis=-1)
        partial_value = jnp.einsum(
            "kgts,skd->tkgd",
            weights.astype(jnp.bfloat16),
            key_block[:, :, 1],
            preferred_element_type=jnp.float32,
        )
        accum = accum * jnp.transpose(shrink, (2, 0, 1))[..., None] + partial_value
        return ((new_max, totals, accum), None)

    result, _ = lax.scan(absorb_advance, (start_max, start_sum, start_acc), blocks)
    maxima, totals, accum = result
    attn_heads = (accum / jnp.transpose(totals, (2, 0, 1))[..., None]).astype(jnp.bfloat16)
    delta_sum = jnp.sum(grad_heads.astype(jnp.float32) * attn_heads.astype(jnp.float32), axis=-1)
    delta_sum = jnp.transpose(delta_sum, (1, 2, 0))
    all_rows = own_pairs.shape[0] * lax.axis_size("sp")
    start_grad = jnp.zeros((row_count, key_count, group_size, HD), jnp.float32)
    start_pairs = jnp.zeros((all_rows, key_count * 2 * HD), jnp.float32)
    blocks, block_size = split_arrived(
        lax.all_gather(own_pairs, "sp", axis=0, tiled=True), key_count
    )

    def collect_advance(status, bundle):
        query_grad, pair_store = status
        key_block, position = bundle
        scores = score_block(queries, key_block, score_scale)
        attend = jnp.exp(scores - maxima[..., None]) / totals[..., None]
        grad_attend = jnp.einsum(
            "tkgd,skd->kgts", grad_heads, key_block[:, :, 1], preferred_element_type=jnp.float32
        )
        mixed = (attend * (grad_attend - delta_sum[..., None]) * score_scale).astype(jnp.bfloat16)
        query_grad = query_grad + jnp.einsum(
            "kgts,skd->tkgd", mixed, key_block[:, :, 0], preferred_element_type=jnp.float32
        )
        grad_key = jnp.einsum("kgts,tkgd->skd", mixed, queries, preferred_element_type=jnp.float32)
        grad_value = jnp.einsum(
            "kgts,tkgd->skd",
            attend.astype(jnp.bfloat16),
            grad_heads,
            preferred_element_type=jnp.float32,
        )
        stacked = jnp.stack([grad_key, grad_value], axis=2).reshape(block_size, key_count * 2 * HD)
        where_rows = position * block_size
        pair_store = lax.dynamic_update_slice_in_dim(pair_store, stacked, where_rows, 0)
        return ((query_grad, pair_store), None)

    positions = jnp.arange(blocks.shape[0], dtype=jnp.int32)
    result, _ = lax.scan(collect_advance, (start_grad, start_pairs), (blocks, positions))
    query_grad, pair_store = result
    pair_grads = lax.psum_scatter(
        pair_store.astype(jnp.bfloat16), "sp", scatter_dimension=0, tiled=True
    )
    grad_query = query_grad.astype(jnp.bfloat16).reshape(row_count, query_count * HD)
    pair_rows = lax.all_to_all(pair_grads, "tp", split_axis=0, concat_axis=1, tiled=True)
    grad_sn = lax.dot_general(pair_rows, w_both, contract_last, preferred_element_type=jnp.float32)
    grad_source = norm_back(source, gain_source, grad_sn)
    attention = attn_heads.reshape(row_count, query_count * HD)
    proj_part = lax.dot_general(
        attention, gathered_grad, (((0,), (0,)), ((), ())), preferred_element_type=jnp.float32
    )
    grad_out_proj = lax.psum(proj_part.astype(jnp.bfloat16), "sp").astype(jnp.float32)
    grad_xn = lax.psum_scatter(
        lax.dot_general(
            grad_query, w_query, contract_last, preferred_element_type=jnp.float32
        ).astype(jnp.bfloat16),
        "tp",
        scatter_dimension=0,
        tiled=True,
    ).astype(jnp.float32)
    grad_target = norm_back(target, gain_target, grad_xn)
    return (grad_target, grad_source, grad_out_proj)


def solution(mesh):
    return jax.shard_map(
        shards,
        mesh=mesh,
        in_specs=(
            P(("sp", "tp"), None),
            P(("sp", "tp"), None),
            P(),
            P(),
            P(None, "tp"),
            P(),
            P(),
            P("tp", None),
            P(("sp", "tp"), None),
        ),
        out_specs=(P(("sp", "tp"), None), P(("sp", "tp"), None), P("tp", None)),
        check_vma=False,
    )
```

profile of v0, /device:TPU:0, one launch (start us, length us, event | category | flops | bytes accessed | tf_op | source)
XLA Modules:
  0.0 473.2 jit_solution(16521432054210177134)
XLA Ops:
  7.2 1.6 fusion.55
  8.8 6.5 %copy.31 = bf16[4096,512]{0,1:T(8,128)(2,1)} copy(bf16[4096,512]{1,0:T(8,128)(2,1)} %param.18) | data formatting | bytes 8388608 | tf_op args[5]
  15.3 6.4 %copy.32 = bf16[4096,512]{0,1:T(8,128)(2,1)} copy(bf16[4096,512]{1,0:T(8,128)(2,1)} %param.19) | data formatting | bytes 8388608 | tf_op args[6]
  21.7 7.4 %pad_maximum_fusion.1 = bf16[4096,8,2,64]{0,3,1,2:T(8,128)(2,1)} fusion(bf16[4096,8,1,64]{0,3,1,2:T(8,128)(2,1)} %bitcast.250, bf16[4096,8,1,64]{0,3,1,2:T(8,128)(2,1)} %bitcast.249), kind=kLoop, calls=%fused_computation.49 | loop fusion | flops 4194304 | bytes 16777216 | tf_op jit(solution)/shard_map/stack | solution.py:69
  29.1 7.8 %copy.33 = bf16[4096,8,2,64]{0,3,2,1:T(8,128)(2,1)} copy(bf16[4096,8,2,64]{0,3,1,2:T(8,128)(2,1)} %pad_maximum_fusion.1) | data formatting | bytes 16777216 | tf_op jit(solution)/shard_map/stack | solution.py:69
  37.0 6.4 %fusion.59 = bf16[16,8,8,128]{3,2,1,0:T(8,128)(2,1)S(1)} fusion(bf16[4096,1024]{0,1:T(8,128)(2,1)} %bitcast.246, bf16[128,4096]{1,0:T(8,128)(2,1)S(1)} %copy-done.1, f32[4096]{0:T(1024)S(1)} %copy-done.6, f32[128]{0:T(128)S(1)} %add_rsqrt_fusion), kind=kOutput, calls=%fused_computation.75 | convolution fusion | flops 1075970048 | bytes 9716224 | tf_op jit(solution)/shard_map/dot_general | solution.py:73
  43.4 12.0 %all_to_all.38 = bf16[128,8,128]{2,0,1:T(8,128)(2,1)} all-to-all(bf16[128,8,128]{2,0,1:T(8,128)(2,1)S(1)} %bitcast.259), channel_id=1, replica_groups=mesh['sp'=16,'tp'=8] {'tp'}, dimensions={1} | all-to-all | bytes 524288 | tf_op jit(solution)/shard_map/all_to_all | solution.py:74
  55.9 1.0 pad_maximum_fusion.2
  57.3 50.2 %all-gather.3.cloned.1.call-done = bf16[16384,128]{1,0:T(8,128)(2,1)} async-done(((bf16[1024,128]{1,0:T(8,128)(2,1)}), bf16[16384,128]{1,0:T(8,128)(2,1)}) %all-gather.3.cloned.1.call-update) | async-done | bytes 4194320 | tf_op jit(solution)/shard_map/all_gather | solution.py:107
  107.4 14.7 %reshape.168 = bf16[16,1024,1,2,64]{4,3,1,0,2:T(2,128)(2,1)} reshape(bf16[16384,128]{1,0:T(8,128)(2,1)} %all-gather.3.cloned.1.call-done) | data formatting | bytes 8388608 | tf_op jit(solution)/shard_map/reshape | solution.py:46
  122.1 20.3 %copy.37 = bf16[16,1024,1,2,64]{1,4,3,2,0:T(8,128)(2,1)} copy(bf16[16,1024,1,2,64]{4,3,1,0,2:T(2,128)(2,1)} %reshape.168) | data formatting | bytes 8388608
  142.4 16.5 %all-gather.5.cloned.1.call-done = bf16[512,8192]{1,0:T(8,128)(2,1)} async-done(((bf16[64,8192]{1,0:T(8,128)(2,1)}), bf16[512,8192]{1,0:T(8,128)(2,1)}) %all-gather.5.cloned.1.call-update) | async-done | bytes 8388624 | tf_op jit(solution)/shard_map/all_gather | solution.py:13
  159.0 3.7 fusion.63
  162.7 54.3 %while.28 = (s32[]{:T(128)}, f32[1,2,512]{2,1,0:T(2,128)S(1)}, f32[1,2,512]{2,1,0:T(2,128)S(1)}, f32[512,1,2,64]{0,3,2,1:T(8,128)S(1)}, bf16[16,1024,1,2,64]{1,4...) while((s32[]{:T(128)}, f32[1,2,512]{2,1,0:T(2,128)S(1)}, ...), condition=%wide.region_5.6_spmd.clone, body=%wide.region_2.5_spmd.clone.sunk | while | flops 277026816 | bytes 14090349 | solution.py:98
  176.3 1.0 dynamic-slice_bitcast_fusion.4
  179.7 1.0 dynamic-slice_bitcast_fusion.4
  217.0 4.0 fusion.60
  221.1 3.9 convolution_convert_fusion.1
  225.0 2.2 broadcast_in_dim.6.clone
  227.3 110.4 %while.29 = (s32[]{:T(128)}, f32[512,1,2,64]{0,3,2,1:T(8,128)S(1)}, bf16[16384,128]{1,0:T(8,128)(2,1)}, bf16[16,1024,1,2,64]{1,4,3,2,0:T(8,128)(2,1)}, bf16[512,...) while((s32[]{:T(128)}, f32[512,1,2,64]{0,3,2,1:T(8,128)S(1)}, ...), condition=%wide.region_8.9_spmd.clone, body=%wide.region_7.8_spmd.clone.sunk | while | flops 679739392 | bytes 22687960 | solution.py:135
  270.8 1.0 fusion.110
  276.8 1.0 dynamic-slice_bitcast_fusion.5
  297.5 1.0 dynamic-slice_bitcast_fusion.5
  337.8 3.3 convolution_convert_fusion
  341.1 2.8 convert_element_type.82
  343.9 72.7 %reduce-scatter.5.cloned.1.call-done = bf16[1024,128]{1,0:T(8,128)(2,1)} async-done(((bf16[16384,128]{1,0:T(8,128)(2,1)}), bf16[1024,128]{1,0:T(8,128)(2,1)}) %reduce-scatter.5.cloned.1.call-update) | async-done | bytes 262160 | tf_op jit(solution)/shard_map/reduce_scatter | solution.py:137
  416.7 4.3 all-to-all-start.1
  421.0 35.0 %reduce-scatter.3.cloned.1.call-done = bf16[64,4096]{1,0:T(8,128)(2,1)} async-done(((bf16[512,4096]{1,0:T(8,128)(2,1)}), bf16[64,4096]{1,0:T(8,128)(2,1)}) %reduce-scatter.3.cloned.1.call-update) | async-done | bytes 524304 | tf_op jit(solution)/shard_map/reduce_scatter | solution.py:149
  456.0 1.3 fusion.71
  457.3 2.4 fusion.69
  459.9 4.9 %fusion.56 = (f32[128]{0:T(128)S(1)}, f32[128,4096]{1,0:T(8,128)S(1)}) fusion(bf16[128,4096]{1,0:T(8,128)(2,1)S(1)} %copy-done.1, f32[4096]{0:T(1024)S(1)} %copy-done.6, bf16[128,1024]{0,1:T(8,128)(2,1)S(1)} %bitcast.256, bf16[4096,1024]{0,1:T(8,128)(2,1)} %bitcast.247), kind=kOutput, calls=%fused_computation.68 | convolution fusion | flops 1075838848 | bytes 11813376 | tf_op jit(solution)/shard_map/dot_general | solution.py:142
  464.8 1.9 fusion.54
  (308 shorter events, 149.1 us)
Async XLA Ops:
  7.2 151.8 %copy-start = (bf16[4096,128]{1,0:T(8,128)(2,1)S(1)}, bf16[4096,128]{1,0:T(8,128)(2,1)}, u32[]{:S(2)}) copy-start(bf16[4096,128]{1,0:T(8,128)(2,1)} %param.17) | copy-start | bytes 3145732
  7.2 100.2 %all-gather.3.cloned.1.call-start = ((), (), s32[]{:S(2)}) async-start(), calls=%async_computation.4 | async-start | bytes 4456448 | tf_op jit(solution)/shard_map/all_gather | solution.py:107
  29.1 7.8 %copy-start.1 = (bf16[128,4096]{1,0:T(8,128)(2,1)S(1)}, bf16[128,4096]{1,0:T(8,128)(2,1)}, u32[]{:S(2)}) copy-start(bf16[128,4096]{1,0:T(8,128)(2,1)} %param.14) | copy-start | bytes 3145732
  29.1 7.8 %copy-start.6 = (f32[4096]{0:T(1024)S(1)}, f32[4096]{0:T(1024)}, u32[]{:S(2)}) copy-start(f32[4096]{0:T(1024)} %param.16) | copy-start | bytes 49156
  36.9 18.5 %copy-start.2 = (bf16[64,4096]{1,0:T(8,128)(2,1)S(1)}, bf16[64,4096]{1,0:T(8,128)(2,1)}, u32[]{:S(2)}) copy-start(bf16[64,4096]{1,0:T(8,128)(2,1)} %param.13) | copy-start | bytes 1572868
  36.9 18.8 %copy-start.5 = (f32[4096]{0:T(1024)S(1)}, f32[4096]{0:T(1024)}, u32[]{:S(2)}) copy-start(f32[4096]{0:T(1024)} %param.15) | copy-start | bytes 49156
  36.9 19.0 %copy-start.4 = (bf16[64,4096]{1,0:T(8,128)(2,1)S(1)}, bf16[64,4096]{1,0:T(8,128)(2,1)}, u32[]{:S(2)}) copy-start(bf16[64,4096]{1,0:T(8,128)(2,1)} %param.21) | copy-start | bytes 1572868
  55.4 103.6 %all-gather.5.cloned.1.call-start = ((), (), s32[]{:S(2)}) async-start(), calls=%async_computation.5 | async-start | bytes 9437184 | tf_op jit(solution)/shard_map/all_gather | solution.py:13
  57.0 284.1 %all-reduce.2.cloned.1.call-start = ((), (), s32[]{:S(2)}) async-start(), calls=%async_computation.8 | async-start | bytes 2097152 | tf_op jit(solution)/shard_map/psum | solution.py:148
  225.0 191.7 %reduce-scatter.5.cloned.1.call-start = ((), (), s32[]{:S(2)}) async-start(), calls=%async_computation.7 | async-start | bytes 4456448 | tf_op jit(solution)/shard_map/reduce_scatter | solution.py:137
  337.7 118.2 %reduce-scatter.3.cloned.1.call-start = ((), (), s32[]{:S(2)}) async-start(), calls=%async_computation.6 | async-start | bytes 4718592 | tf_op jit(solution)/shard_map/reduce_scatter | solution.py:149
  341.1 114.9 %copy-start.3 = (bf16[64,4096]{1,0:T(8,128)(2,1)S(1)}, bf16[64,4096]{1,0:T(8,128)(2,1)}, u32[]{:S(2)}) copy-start(bf16[64,4096]{1,0:T(8,128)(2,1)} %param.13) | copy-start | bytes 1572868
  416.7 43.0 %all-to-all-start.1 = ((bf16[8,128,128]{2,1,0:T(8,128)(2,1)}), bf16[8,128,128]{2,1,0:T(8,128)(2,1)S(1)}, u32[]{:S(2)}, u32[]{:S(2)}) async-start(bf16[8,128,128]{2,1,0:T(8,128)(2,1)} %bitcast.262), calls=%async_computation.3 | async-start | bytes 524288 | tf_op jit(solution)/shard_map/all_to_all | solution.py:141
Sparse Core Ops, SparseCore 0:
  55.5 51.8 all-gather.2
  109.7 49.2 all-gather.4
  225.1 87.6 all-reduce.1
  337.9 78.7 reduce-scatter.4
  418.9 37.0 reduce-scatter.2
where the time goes:
time: 476 us; the launch traced here: 473 us
  waiting for transfers between devices  175 us (37%)
  local copies, waits for them, and re-layouts  113 us (24%)
  matrix products  112 us (24%)
  other arithmetic  31.2 us (7%)
  between operations  14 us (3%)
  blocking collectives  12 us (3%)
  loops' own time  12 us (3%)
    reduce_scatter x1, waiting for transfers between devices, shards(): lax.psum_scatter(pair_store.astype(jnp.bfloat16), 'sp', scatter_dimension...  72.7 us
    all_gather x1, waiting for transfers between devices, shards(): lax.all_gather(own_pairs, 'sp', axis=0, tiled=True)  50.2 us
    reduce_scatter x1, waiting for transfers between devices, shards(): lax.psum_scatter(lax.dot_general(grad_query, w_query, contract_last, pref...  35 us
    unnamed x17, local copies, waits for them, and re-layouts  33.2 us
    squeeze x32, local copies, waits for them, and re-layouts, shards(): lax.scan(absorb_advance, (start_max, start_sum, start_acc), blocks)  31.2 us
    dot_general x32, matrix products, score_block(): jnp.einsum('tkgd,skd->kgts', queries, key_block[:, :, 0], preferred_eleme...  27.3 us
    all_gather x1, waiting for transfers between devices, sent_together(): lax.all_gather(both, axis, axis=dim, tiled=True)  16.5 us
    reshape x1, local copies, waits for them, and re-layouts, split_arrived(): arrived.reshape(row_count // block_size, block_size, key_count, 2, HD)  14.7 us
  transfers between devices with their start and end apart: 6, of which 4 were waited for; matrix products, arithmetic and copies ran while one was open for 31% of the time, Pallas kernels for 0%

commit v1 on v0

--- a/solution.py
+++ b/solution.py
@@ -6,6 +6,19 @@
 
 HD = 64
 EPS = 1e-06
+
+
+def collect(x, axis, dim):
+    ways = lax.axis_size(axis)
+    up = [(d, (d + 1) % ways) for d in range(ways)]
+    down = [(d, (d - 1) % ways) for d in range(ways)]
+    earlier, later = ([x], [x])
+    for _ in range(ways // 2):
+        earlier.append(lax.ppermute(earlier[-1], axis, up))
+    for _ in range((ways - 1) // 2):
+        later.append(lax.ppermute(later[-1], axis, down))
+    line = jnp.concatenate([*earlier[::-1], *later[1:]], axis=dim)
+    return jnp.roll(line, (lax.axis_index(axis) - ways // 2) * x.shape[dim], axis=dim)
 
 
 def sent_together(arrays, axis, dim, along):
@@ -103,9 +116,7 @@
     all_rows = own_pairs.shape[0] * lax.axis_size("sp")
     start_grad = jnp.zeros((row_count, key_count, group_size, HD), jnp.float32)
     start_pairs = jnp.zeros((all_rows, key_count * 2 * HD), jnp.float32)
-    blocks, block_size = split_arrived(
-        lax.all_gather(own_pairs, "sp", axis=0, tiled=True), key_count
-    )
+    blocks, block_size = split_arrived(collect(own_pairs, "sp", 0), key_count)
 
     def collect_advance(status, bundle):
         query_grad, pair_store = status

time: 476 us -> 788 us (1.66)
  matrix products: 112 us -> 246 us
  local copies, waits for them, and re-layouts: 113 us -> 214 us
  other arithmetic: 31.2 us -> 77.1 us
  starting transfers between devices: 4.68 us -> 44.8 us
  waiting for transfers between devices: 175 us -> 160 us
    dot_general x32, matrix products: 27.3 us -> 87.3 us  [score_block(): jnp.einsum('tkgd,skd->kgts', queries, key_block[:, :, 0], preferred_eleme...]
    ppermute x0 -> x15, waiting for transfers between devices: none -> 56.6 us  [the longest x8 49.5 us: collect(): earlier.append(lax.ppermute(earlier[-1], axis, up))]
    all_gather x1, waiting for transfers between devices: 50.2 us -> 0.01 us  [shards(): lax.all_gather(own_pairs, 'sp', axis=0, tiled=True)]
    dynamic_update_slice x32, local copies, waits for them, and re-layouts: 14.4 us -> 55.7 us  [collect_advance(): lax.dynamic_update_slice_in_dim(pair_store, stacked, where_rows, 0)]
    ppermute x0 -> x15, starting transfers between devices: none -> 40.1 us  [the longest x7 38.5 us: collect(): later.append(lax.ppermute(later[-1], axis, down))]
    reduce_sum x16, other arithmetic: 11.2 us -> 46.2 us  [absorb_advance(): totals = totals * shrink + jnp.sum(weights, axis=-1)]
    dot_general x16, matrix products: 14.2 us -> 49.1 us  [absorb_advance(): jnp.einsum('kgts,skd->tkgd', weights.astype(jnp.bfloat16), key_block[:, :...]
    unnamed x17 -> x75, local copies, waits for them, and re-layouts: 33.2 us -> 65 us
  transfers between devices with their start and end apart: 6 -> 21, of which waited for: 4 -> 12; matrix products, arithmetic and copies ran while one was open for 31% -> 40% of each run, Pallas kernels for 0% -> 0%
where the time goes in v1:
time: 788 us; the launch traced here: 780 us
  matrix products  246 us (31%)
  local copies, waits for them, and re-layouts  214 us (27%)
  waiting for transfers between devices  160 us (20%)
  other arithmetic  77.1 us (10%)
  starting transfers between devices  44.8 us (6%)
  between operations  14.3 us (2%)
  blocking collectives  12 us (2%)
  loops' own time  11.5 us (1%)
    dot_general x32, matrix products, score_block(): jnp.einsum('tkgd,skd->kgts', queries, key_block[:, :, 0], preferred_eleme...  87.3 us
    reduce_scatter x1, waiting for transfers between devices, shards(): lax.psum_scatter(pair_store.astype(jnp.bfloat16), 'sp', scatter_dimension...  67.9 us
    unnamed x75, local copies, waits for them, and re-layouts  65 us
    dynamic_update_slice x32, local copies, waits for them, and re-layouts, collect_advance(): lax.dynamic_update_slice_in_dim(pair_store, stacked, where_rows, 0)  55.7 us
    ppermute x8, waiting for transfers between devices, collect(): earlier.append(lax.ppermute(earlier[-1], axis, up))  49.5 us
    dot_general x16, matrix products, absorb_advance(): jnp.einsum('kgts,skd->tkgd', weights.astype(jnp.bfloat16), key_block[:, :...  49.1 us
    reduce_sum x16, other arithmetic, absorb_advance(): totals = totals * shrink + jnp.sum(weights, axis=-1)  46.2 us
    ppermute x7, starting transfers between devices, collect(): later.append(lax.ppermute(later[-1], axis, down))  38.5 us
  transfers between devices with their start and end apart: 21, of which 12 were waited for; matrix products, arithmetic and copies ran while one was open for 40% of the time, Pallas kernels for 0%

profile of v1, /device:TPU:0, one launch (start us, length us, event | category | flops | bytes accessed | tf_op | source)
XLA Modules:
  0.0 780.3 jit_solution(10027543036886974027)
XLA Ops:
  7.2 6.6 copy.32
  13.8 6.4 copy.33
  20.2 7.4 pad_maximum_fusion.1
  27.7 7.9 %copy.34 = bf16[4096,8,2,64]{0,3,2,1:T(8,128)(2,1)} copy(bf16[4096,8,2,64]{0,3,1,2:T(8,128)(2,1)} %pad_maximum_fusion.1) | data formatting | bytes 16777216 | tf_op jit(solution)/shard_map/stack | solution.py:82
  35.8 6.3 fusion.59
  42.2 12.0 %all_to_all.38 = bf16[128,8,128]{2,0,1:T(8,128)(2,1)} all-to-all(bf16[128,8,128]{2,0,1:T(8,128)(2,1)S(1)} %bitcast.262), channel_id=1, replica_groups=mesh['sp'=16,'tp'=8] {'tp'}, dimensions={1} | all-to-all | bytes 524288 | tf_op jit(solution)/shard_map/all_to_all | solution.py:87
  57.4 10.9 %collective-permute-done = bf16[1024,128]{1,0:T(8,128)(2,1)S(1)} collective-permute-done((bf16[1024,128]{1,0:T(8,128)(2,1)}, bf16[1024,128]{1,0:T(8,128)(2,1)S(1)}, u32[]{:S(2)}, u32[]{:S(2)}) %collective-permute-start) | collective-permute-done | bytes 262176 | tf_op jit(solution)/shard_map/ppermute | solution.py:17
  68.3 5.3 collective-permute-start.8
  73.7 7.9 %collective-permute-done.1 = bf16[1024,128]{1,0:T(8,128)(2,1)S(1)} collective-permute-done((bf16[1024,128]{1,0:T(8,128)(2,1)S(1)}, bf16[1024,128]{1,0:T(8,128)(2,1)S(1)}, u32[]{:S(2)}, u32[]{:S(2)}) %collective-permute-start.1) | collective-permute-done | bytes 262176 | tf_op jit(solution)/shard_map/ppermute | solution.py:17
  81.6 5.3 collective-permute-start.9
  86.9 5.3 collective-permute-done.2
  92.2 4.3 collective-permute-done.9
  96.5 5.8 collective-permute-start.10
  102.3 7.1 collective-permute-done.3
  112.2 5.8 collective-permute-start.11
  118.0 4.4 collective-permute-done.4
  122.4 5.3 collective-permute-start.12
  127.8 5.2 collective-permute-done.5
  133.0 5.3 collective-permute-start.13
  138.3 4.4 collective-permute-done.6
  142.8 5.5 collective-permute-start.14
  148.4 4.4 collective-permute-done.7
  166.9 14.8 %reshape.171 = bf16[16,1024,1,2,64]{4,3,1,0,2:T(2,128)(2,1)} reshape(bf16[16384,128]{1,0:T(8,128)(2,1)} %constant_dynamic-slice_fusion) | data formatting | bytes 8388608 | tf_op jit(solution)/shard_map/reshape | solution.py:59
  181.6 20.1 %copy.39 = bf16[16,1024,1,2,64]{1,4,3,2,0:T(8,128)(2,1)} copy(bf16[16,1024,1,2,64]{4,3,1,0,2:T(2,128)(2,1)} %reshape.171) | data formatting | bytes 8388608
  201.7 14.8 %reshape.172 = bf16[16,1024,1,2,64]{4,3,1,0,2:T(2,128)(2,1)} reshape(bf16[16384,128]{1,0:T(8,128)(2,1)} %all-gather.5.cloned.1.call-done) | data formatting | bytes 8388608 | tf_op jit(solution)/shard_map/reshape | solution.py:59
  216.5 20.2 %copy.38 = bf16[16,1024,1,2,64]{1,4,3,2,0:T(8,128)(2,1)} copy(bf16[16,1024,1,2,64]{4,3,1,0,2:T(2,128)(2,1)} %reshape.172) | data formatting | bytes 8388608
  236.7 4.4 fusion.63
  241.0 169.4 %while.28 = (s32[]{:T(128)}, f32[1,2,512]{2,1,0:T(2,128)S(1)}, f32[1,2,512]{2,1,0:T(2,128)S(1)}, f32[512,1,2,64]{0,3,2,1:T(8,128)S(1)}, bf16[16,1024,1,2,64]{1,4...) while((s32[]{:T(128)}, f32[1,2,512]{2,1,0:T(2,128)S(1)}, ...), condition=%wide.region_5.6_spmd.clone, body=%wide.region_2.5_spmd.clone.sunk | while | flops 277026816 | bytes 14090341 | solution.py:111
  421.3 227.2 %while.29 = (s32[]{:T(128)}, f32[512,1,2,64]{0,3,2,1:T(8,128)}, bf16[16384,128]{1,0:T(8,128)(2,1)}, bf16[16,1024,1,2,64]{1,4,3,2,0:T(8,128)(2,1)}, bf16[512,1,2,...) while((s32[]{:T(128)}, f32[512,1,2,64]{0,3,2,1:T(8,128)}, ...), condition=%wide.region_8.9_spmd.clone, body=%wide.region_7.8_spmd.clone.sunk | while | flops 679739392 | bytes 22687952 | solution.py:146
  655.7 67.9 %reduce-scatter.5.cloned.1.call-done = bf16[1024,128]{1,0:T(8,128)(2,1)} async-done(((bf16[16384,128]{1,0:T(8,128)(2,1)}), bf16[1024,128]{1,0:T(8,128)(2,1)}) %reduce-scatter.5.cloned.1.call-update) | async-done | bytes 262160 | tf_op jit(solution)/shard_map/reduce_scatter | solution.py:148
  727.9 35.1 %reduce-scatter.3.cloned.1.call-done = bf16[64,4096]{1,0:T(8,128)(2,1)} async-done(((bf16[512,4096]{1,0:T(8,128)(2,1)}), bf16[64,4096]{1,0:T(8,128)(2,1)}) %reduce-scatter.3.cloned.1.call-update) | async-done | bytes 524304 | tf_op jit(solution)/shard_map/reduce_scatter | solution.py:160
  766.9 4.9 fusion.56
  (399 shorter events, 433.4 us)
Async XLA Ops:
  7.2 229.5 %copy-start = (bf16[4096,128]{1,0:T(8,128)(2,1)S(1)}, bf16[4096,128]{1,0:T(8,128)(2,1)}, u32[]{:S(2)}) copy-start(bf16[4096,128]{1,0:T(8,128)(2,1)} %param.17) | copy-start | bytes 3145732
  7.2 194.6 %all-gather.5.cloned.1.call-start = ((), (), s32[]{:S(2)}) async-start(), calls=%async_computation.5 | async-start | bytes 4456448 | tf_op jit(solution)/shard_map/all_gather | solution.py:92
  54.2 103.6 %copy-start.5 = (bf16[128,8,128]{2,0,1:T(8,128)(2,1)S(1)}, bf16[128,8,128]{2,0,1:T(8,128)(2,1)}, u32[]{:S(2)}) copy-start(bf16[128,8,128]{2,0,1:T(8,128)(2,1)} %all_to_all.38) | copy-start | bytes 786436
  54.3 182.4 %all-gather.3.cloned.1.call-start = ((), (), s32[]{:S(2)}) async-start(), calls=%async_computation.4 | async-start | bytes 9437184 | tf_op jit(solution)/shard_map/all_gather | solution.py:26
  54.5 27.0 %copy-start.17 = (f32[64]{0:T(128)}, f32[64]{0:T(128)S(1)}, u32[]{:S(2)}) copy-start(f32[64]{0:T(128)S(1)} %add_rsqrt_fusion.1) | copy-start | bytes 772
  55.8 597.1 %all-reduce.2.cloned.1.call-start = ((), (), s32[]{:S(2)}) async-start(), calls=%async_computation.8 | async-start | bytes 2097152 | tf_op jit(solution)/shard_map/psum | solution.py:159
  55.9 12.4 %collective-permute-start = (bf16[1024,128]{1,0:T(8,128)(2,1)}, bf16[1024,128]{1,0:T(8,128)(2,1)S(1)}, u32[]{:S(2)}, u32[]{:S(2)}) collective-permute-start(bf16[1024,128]{1,0:T(8,128)(2,1)} %bitcast.254), channel_id=1, source_target_pairs={{0,8},{8,16},{16,24},{24,32},{32,40},{40,48},{48,56},{56,64},{64,7... | collective-permute-start | bytes 786440 | tf_op jit(solution)/shard_map/ppermute | solution.py:17
  68.3 13.2 %collective-permute-start.1 = (bf16[1024,128]{1,0:T(8,128)(2,1)S(1)}, bf16[1024,128]{1,0:T(8,128)(2,1)S(1)}, u32[]{:S(2)}, u32[]{:S(2)}) collective-permute-start(bf16[1024,128]{1,0:T(8,128)(2,1)S(1)} %collective-permute-done), channel_id=1, source_target_pairs={{0,8},{8,16},{16,24},{24,32},{32,40},{40,48},{48,56},{56,64},{64,7... | collective-permute-start | bytes 786440 | tf_op jit(solution)/shard_map/ppermute | solution.py:17
  68.3 13.2 %collective-permute-start.8 = (bf16[1024,128]{1,0:T(8,128)(2,1)}, bf16[1024,128]{1,0:T(8,128)(2,1)S(1)}, u32[]{:S(2)}, u32[]{:S(2)}) collective-permute-start(bf16[1024,128]{1,0:T(8,128)(2,1)} %bitcast.255), channel_id=1, source_target_pairs={{0,120},{8,0},{16,8},{24,16},{32,24},{40,32},{48,40},{56,48},{64,5... | collective-permute-start | bytes 786440 | tf_op jit(solution)/shard_map/ppermute | solution.py:19
  81.6 10.6 %collective-permute-start.2 = (bf16[1024,128]{1,0:T(8,128)(2,1)S(1)}, bf16[1024,128]{1,0:T(8,128)(2,1)S(1)}, u32[]{:S(2)}, u32[]{:S(2)}) collective-permute-start(bf16[1024,128]{1,0:T(8,128)(2,1)S(1)} %collective-permute-done.1), channel_id=1, source_target_pairs={{0,8},{8,16},{16,24},{24,32},{32,40},{40,48},{48,56},{56,64},{64,7... | collective-permute-start | bytes 786440 | tf_op jit(solution)/shard_map/ppermute | solution.py:17
  81.6 14.9 %collective-permute-start.9 = (bf16[1024,128]{1,0:T(8,128)(2,1)S(1)}, bf16[1024,128]{1,0:T(8,128)(2,1)S(1)}, u32[]{:S(2)}, u32[]{:S(2)}) collective-permute-start(bf16[1024,128]{1,0:T(8,128)(2,1)S(1)} %collective-permute-done.8), channel_id=1, source_target_pairs={{0,120},{8,0},{16,8},{24,16},{32,24},{40,32},{48,40},{56,48},{64,5... | collective-permute-start | bytes 786440 | tf_op jit(solution)/shard_map/ppermute | solution.py:19
  92.2 17.3 %collective-permute-start.3 = (bf16[1024,128]{1,0:T(8,128)(2,1)S(1)}, bf16[1024,128]{1,0:T(8,128)(2,1)S(1)}, u32[]{:S(2)}, u32[]{:S(2)}) collective-permute-start(bf16[1024,128]{1,0:T(8,128)(2,1)S(1)} %collective-permute-done.2), channel_id=1, source_target_pairs={{0,8},{8,16},{16,24},{24,32},{32,40},{40,48},{48,56},{56,64},{64,7... | collective-permute-start | bytes 786440 | tf_op jit(solution)/shard_map/ppermute | solution.py:17
  96.5 15.7 %collective-permute-start.10 = (bf16[1024,128]{1,0:T(8,128)(2,1)S(1)}, bf16[1024,128]{1,0:T(8,128)(2,1)S(1)}, u32[]{:S(2)}, u32[]{:S(2)}) collective-permute-start(bf16[1024,128]{1,0:T(8,128)(2,1)S(1)} %collective-permute-done.9), channel_id=1, source_target_pairs={{0,120},{8,0},{16,8},{24,16},{32,24},{40,32},{48,40},{56,48},{64,5... | collective-permute-start | bytes 786440 | tf_op jit(solution)/shard_map/ppermute | solution.py:19
  109.4 33.3 %copy-start.6 = (bf16[1024,128]{1,0:T(8,128)(2,1)}, bf16[1024,128]{1,0:T(8,128)(2,1)S(1)}, u32[]{:S(2)}) copy-start(bf16[1024,128]{1,0:T(8,128)(2,1)S(1)} %collective-permute-done.3) | copy-start | bytes 786436
  109.4 13.0 %collective-permute-start.4 = (bf16[1024,128]{1,0:T(8,128)(2,1)S(1)}, bf16[1024,128]{1,0:T(8,128)(2,1)S(1)}, u32[]{:S(2)}, u32[]{:S(2)}) collective-permute-start(bf16[1024,128]{1,0:T(8,128)(2,1)S(1)} %collective-permute-done.3), channel_id=1, source_target_pairs={{0,8},{8,16},{16,24},{24,32},{32,40},{40,48},{48,56},{56,64},{64,7... | collective-permute-start | bytes 786440 | tf_op jit(solution)/shard_map/ppermute | solution.py:17
  112.2 10.2 %collective-permute-start.11 = (bf16[1024,128]{1,0:T(8,128)(2,1)S(1)}, bf16[1024,128]{1,0:T(8,128)(2,1)S(1)}, u32[]{:S(2)}, u32[]{:S(2)}) collective-permute-start(bf16[1024,128]{1,0:T(8,128)(2,1)S(1)} %collective-permute-done.10), channel_id=1, source_target_pairs={{0,120},{8,0},{16,8},{24,16},{32,24},{40,32},{48,40},{56,48},{64,5... | collective-permute-start | bytes 786440 | tf_op jit(solution)/shard_map/ppermute | solution.py:19
  122.4 10.5 %collective-permute-start.5 = (bf16[1024,128]{1,0:T(8,128)(2,1)S(1)}, bf16[1024,128]{1,0:T(8,128)(2,1)S(1)}, u32[]{:S(2)}, u32[]{:S(2)}) collective-permute-start(bf16[1024,128]{1,0:T(8,128)(2,1)S(1)} %collective-permute-done.4), channel_id=1, source_target_pairs={{0,8},{8,16},{16,24},{24,32},{32,40},{40,48},{48,56},{56,64},{64,7... | collective-permute-start | bytes 786440 | tf_op jit(solution)/shard_map/ppermute | solution.py:17
  122.4 10.5 %collective-permute-start.12 = (bf16[1024,128]{1,0:T(8,128)(2,1)S(1)}, bf16[1024,128]{1,0:T(8,128)(2,1)}, u32[]{:S(2)}, u32[]{:S(2)}) collective-permute-start(bf16[1024,128]{1,0:T(8,128)(2,1)S(1)} %collective-permute-done.11), channel_id=1, source_target_pairs={{0,120},{8,0},{16,8},{24,16},{32,24},{40,32},{48,40},{56,48},{64,5... | collective-permute-start | bytes 786440 | tf_op jit(solution)/shard_map/ppermute | solution.py:19
  132.9 9.8 %collective-permute-start.6 = (bf16[1024,128]{1,0:T(8,128)(2,1)S(1)}, bf16[1024,128]{1,0:T(8,128)(2,1)}, u32[]{:S(2)}, u32[]{:S(2)}) collective-permute-start(bf16[1024,128]{1,0:T(8,128)(2,1)S(1)} %collective-permute-done.5), channel_id=1, source_target_pairs={{0,8},{8,16},{16,24},{24,32},{32,40},{40,48},{48,56},{56,64},{64,7... | collective-permute-start | bytes 786440 | tf_op jit(solution)/shard_map/ppermute | solution.py:17
  133.0 9.9 %collective-permute-start.13 = (bf16[1024,128]{1,0:T(8,128)(2,1)}, bf16[1024,128]{1,0:T(8,128)(2,1)}, u32[]{:S(2)}, u32[]{:S(2)}) collective-permute-start(bf16[1024,128]{1,0:T(8,128)(2,1)} %collective-permute-done.12), channel_id=1, source_target_pairs={{0,120},{8,0},{16,8},{24,16},{32,24},{40,32},{48,40},{56,48},{64,5... | collective-permute-start | bytes 786440 | tf_op jit(solution)/shard_map/ppermute | solution.py:19
  142.7 10.0 %collective-permute-start.7 = (bf16[1024,128]{1,0:T(8,128)(2,1)}, bf16[1024,128]{1,0:T(8,128)(2,1)}, u32[]{:S(2)}, u32[]{:S(2)}) collective-permute-start(bf16[1024,128]{1,0:T(8,128)(2,1)} %collective-permute-done.6), channel_id=1, source_target_pairs={{0,8},{8,16},{16,24},{24,32},{32,40},{40,48},{48,56},{56,64},{64,7... | collective-permute-start | bytes 786440 | tf_op jit(solution)/shard_map/ppermute | solution.py:17
  142.8 19.4 %copy-start.7 = (bf16[1024,128]{1,0:T(8,128)(2,1)S(1)}, bf16[1024,128]{1,0:T(8,128)(2,1)}, u32[]{:S(2)}) copy-start(bf16[1024,128]{1,0:T(8,128)(2,1)} %copy-done.6) | copy-start | bytes 786436
  142.8 17.3 %collective-permute-start.14 = (bf16[1024,128]{1,0:T(8,128)(2,1)}, bf16[1024,128]{1,0:T(8,128)(2,1)S(1)}, u32[]{:S(2)}, u32[]{:S(2)}) collective-permute-start(bf16[1024,128]{1,0:T(8,128)(2,1)} %collective-permute-done.13), channel_id=1, source_target_pairs={{0,120},{8,0},{16,8},{24,16},{32,24},{40,32},{48,40},{56,48},{64,5... | collective-permute-start | bytes 786440 | tf_op jit(solution)/shard_map/ppermute | solution.py:19
  241.0 169.4 %copy-start.19 = (bf16[128,4096]{1,0:T(8,128)(2,1)S(1)}, bf16[128,4096]{1,0:T(8,128)(2,1)}, u32[]{:S(2)}) copy-start(bf16[128,4096]{1,0:T(8,128)(2,1)} %param.20) | copy-start | bytes 3145732
  418.2 305.4 %reduce-scatter.5.cloned.1.call-start = ((), (), s32[]{:S(2)}) async-start(), calls=%async_computation.7 | async-start | bytes 4456448 | tf_op jit(solution)/shard_map/reduce_scatter | solution.py:148
  648.6 114.4 %copy-start.4 = (bf16[64,4096]{1,0:T(8,128)(2,1)S(1)}, bf16[64,4096]{1,0:T(8,128)(2,1)}, u32[]{:S(2)}) copy-start(bf16[64,4096]{1,0:T(8,128)(2,1)} %param.13) | copy-start | bytes 1572868
  648.6 114.4 %copy-start.14 = (f32[4096]{0:T(1024)S(1)}, f32[4096]{0:T(1024)}, u32[]{:S(2)}) copy-start(f32[4096]{0:T(1024)} %param.15) | copy-start | bytes 49156
  648.6 114.4 %reduce-scatter.3.cloned.1.call-start = ((), (), s32[]{:S(2)}) async-start(), calls=%async_computation.6 | async-start | bytes 4718592 | tf_op jit(solution)/shard_map/reduce_scatter | solution.py:160
  648.6 115.7 %copy-start.18 = (f32[64]{0:T(128)S(1)}, f32[64]{0:T(128)}, u32[]{:S(2)}) copy-start(f32[64]{0:T(128)} %copy-done.17) | copy-start | bytes 772
  649.7 117.2 %copy-start.2 = (bf16[128,4096]{1,0:T(8,128)(2,1)S(1)}, bf16[128,4096]{1,0:T(8,128)(2,1)}, u32[]{:S(2)}) copy-start(bf16[128,4096]{1,0:T(8,128)(2,1)} %param.14) | copy-start | bytes 3145732
  649.7 117.2 %copy-start.16 = (f32[4096]{0:T(1024)S(1)}, f32[4096]{0:T(1024)}, u32[]{:S(2)}) copy-start(f32[4096]{0:T(1024)} %param.16) | copy-start | bytes 49156
  723.6 43.1 %all-to-all-start.1 = ((bf16[8,128,128]{2,1,0:T(8,128)(2,1)}), bf16[8,128,128]{2,1,0:T(8,128)(2,1)S(1)}, u32[]{:S(2)}, u32[]{:S(2)}) async-start(bf16[8,128,128]{2,1,0:T(8,128)(2,1)} %bitcast.265), calls=%async_computation.3 | async-start | bytes 524288 | tf_op jit(solution)/shard_map/all_to_all | solution.py:152
  (9 other events, 127.7 us)
Sparse Core Ops, SparseCore 0:
  54.4 65.9 all-gather.4
  122.7 48.8 all-gather.2
  418.3 83.8 all-reduce.1
  648.7 74.8 reduce-scatter.4
  725.9 37.0 reduce-scatter.2
